TPU v7x, 32 devices: a whole 2x2x4 slice. The times are simulated.
32 devices in a mesh: sp: 4 (over z), fs: 4 (over y, x), tp: 2 (over core).
Axes of the slice: x: 2, y: 2, z: 4, core: 2. Of those that a mesh axis runs over, the one named last changes fastest.
Arguments:
- inputs: bfloat16 [4, 512, 2048], P('fs', 'sp', 'tp'), may hold values from -6 to 6
- input_norm_scale: float32 [2048], replicated, may hold values from 0.1 to 1.9
- query_matrix: bfloat16 [2048, 512], P('sp', 'tp'), may hold values from -0.125 to 0.125
- key_matrix: bfloat16 [2048, 512], P('sp', 'tp'), may hold values from -0.125 to 0.125
- value_matrix: bfloat16 [2048, 512], P('sp', 'tp'), may hold values from -0.125 to 0.125
- decay_down_weight: bfloat16 [2048, 128], replicated, may hold values from -0.125 to 0.125
- decay_up_weight: bfloat16 [128, 512], P(None, 'tp'), may hold values from -1.1953125 to 1.1953125
- decay_bias_base: float32 [512], P('tp'), as said below
- decay_position_offset: float32 [4, 512, 8], P('fs', 'sp', 'tp'), may hold values from -0.7 to 0.7
- extra_log_decay: float32 [4, 512, 8], P('fs', 'sp', 'tp'), may hold values from -2.8 to 0, as said below
- correction_down_weight: bfloat16 [2048, 128], replicated, may hold values from -0.125 to 0.125
- correction_up_weight: bfloat16 [128, 512], P(None, 'tp'), may hold values from -1.1953125 to 1.1953125
- correction_rate_bias: float32 [512], P('tp'), as said below
- head_norm_scale: float32 [512], P('tp'), may hold values from 0.1 to 1.9
- starting_states: float32 [4, 2, 8, 64, 64], P('fs', None, 'tp'), may hold values from -128 to 128
- pointwise_value_weight: bfloat16 [2048, 1024], P('sp', 'tp'), may hold values from -0.125 to 0.125
- pointwise_gate_weight: bfloat16 [2048, 1024], P('sp', 'tp'), may hold values from -0.125 to 0.125
- depthwise_taps_weight: float32 [31, 1024], P(None, 'tp')
- channel_norm_scale: float32 [1024], P('tp'), may hold values from 0.1 to 1.9
- mixer_output_weight: bfloat16 [512, 2048], P('tp', 'sp'), may hold values from -0.15625 to 0.15625
- convolution_output_weight: bfloat16 [1024, 2048], P('tp', 'sp'), may hold values from -0.15625 to 0.15625
Outputs:
- mixed: bfloat16 [4, 512, 2048], P('fs', ('sp', 'tp'))
Inputs may be any that keep to these rules, and one draw needn't show every extreme that they name: `decay_bias_base`: decay bases, one value for every channel. `correction_rate_bias`: correction-rate bases, one value for every channel. `extra_log_decay`: zero at all but a few positions of each sequence.
All inputs are finite; a program needn't handle non-finite values.
Results may differ from a plain program's by a relative error of at most 0.012.
Values may be sent and summed in bfloat16 or wider, within the bound.
A program may use at most 64 MiB of HBM per device.

v0:
```python
import functools

import jax
import jax.numpy as jnp
from jax import lax
from jax.experimental import pallas as pl
from jax.experimental.pallas import tpu as pltpu
from jax.sharding import PartitionSpec as P

GROUP = 64
CHUNK = 64
MESH = pl.DeviceIdType.MESH
f32 = jnp.float32
bf16 = jnp.bfloat16
NN = (((1,), (0,)), ((), ()))
NT = (((1,), (1,)), ((), ()))
TN = (((0,), (0,)), ((), ()))


def dot1(a, b, dims=NN):
    return lax.dot_general(a, b, dims, preferred_element_type=f32)


def halves(a):
    hi = a.astype(bf16)
    return hi, (a - hi.astype(f32)).astype(bf16)


def dot3(a, b, dims=NN):
    a, b = (x if isinstance(x, tuple) else halves(x) for x in (a, b))
    return dot1(a[0], b[0], dims) + (dot1(a[0], b[1], dims) + dot1(a[1], b[0], dims))


def exact_left(mask, x):
    hi, rest = x.astype(bf16), x - x.astype(bf16).astype(f32)
    mid, low = halves(rest)
    return dot1(mask, hi) + (dot1(mask, mid) + dot1(mask, low))


def remote(src, dst, send, recv, where):
    return pltpu.make_async_remote_copy(
        src_ref=src, dst_ref=dst, send_sem=send, recv_sem=recv, device_id=where, device_id_type=MESH
    )


def greet(peers):
    barrier = pltpu.get_barrier_semaphore()
    for where in peers:
        pl.semaphore_signal(barrier, inc=1, device_id=where, device_id_type=MESH)
    pl.semaphore_wait(barrier, len(peers))


def collect_kernel(n, m, x_ref, w_ref, e_ref, xo, wo, eo, local, xsend, xrecv, dsend, drecv, wsend, wrecv, esend, erecv):
    s, t = lax.axis_index("sp"), lax.axis_index("tp")
    rows, feats = x_ref.shape
    depth = w_ref.shape[1]

    def slot(b, c):
        return xo.at[pl.ds(b * rows, rows), pl.ds(pl.multiple_of(c * feats, feats), feats)]

    own_x = pltpu.make_async_copy(x_ref, slot(s, t), local.at[0])
    own_w = pltpu.make_async_copy(w_ref.at[s], wo.at[pl.ds(s * depth, depth)], local.at[1])
    own_e = pltpu.make_async_copy(e_ref, eo.at[s], local.at[2])
    for copy in (own_x, own_w, own_e):
        copy.start()
    ring = [lax.rem(s + k, n) for k in range(1, n)]
    mates = [lax.rem(t + k, m) for k in range(1, m)]
    greet([{"sp": p} for p in ring] + [{"tp": c} for c in mates])

    def along(k, way):
        b = s - k if way == 0 else s + k
        src = x_ref if k == 0 else slot(b, t)
        return remote(src, slot(b, t), xsend.at[way, k], xrecv.at[way, k], {"sp": s + 1 if way == 0 else s - 1})

    def sends(k, way):
        return (s - k >= 0) & (s < n - 1) if way == 0 else (s + k < n) & (s > 0)

    def gets(k, way):
        return s - 1 - k >= 0 if way == 0 else s + 1 + k < n

    def across(index, j, b):
        src = x_ref if index == 0 else slot(b, t)
        return remote(src, slot(b, t), dsend.at[index, j], drecv.at[index, j], {"tp": mates[j]})

    def across_in(index, j, b):
        c = lax.rem(t + m - 1 - j, m)
        return remote(slot(b, c), slot(b, c), dsend.at[index, j], drecv.at[index, j], {"tp": mates[j]})

    for way in range(2):
        @pl.when(sends(0, way))
        def _():
            along(0, way).start()
    extras = []
    for k in range(1, n):
        copy = remote(e_ref, eo.at[s], esend.at[k - 1], erecv.at[k - 1], {"sp": ring[k - 1]})
        copy.start()
        extras.append(copy)
    weights = []
    for k in range(1, n):
        p = ring[k - 1]
        copy = remote(
            w_ref.at[p], wo.at[pl.ds(s * depth, depth)], wsend.at[k - 1], wrecv.at[k - 1], {"sp": p}
        )
        copy.start()
        weights.append(copy)
    for j in range(m - 1):
        across(0, j, s).start()
    for k in range(n - 1):
        for way in range(2):
            @pl.when(gets(k, way))
            def _():
                b = s - 1 - k if way == 0 else s + 1 + k
                remote(slot(b, t), slot(b, t), xsend.at[way, k], xrecv.at[way, k], {"sp": b}).wait_recv()
                if k + 1 < n - 1:
                    @pl.when(sends(k + 1, way))
                    def _():
                        along(k + 1, way).start()
                for j in range(m - 1):
                    across(1 + 2 * k + way, j, b).start()
    for j in range(m - 1):
        across_in(0, j, s).wait_recv()
        across(0, j, s).wait_send()
    for k in range(n - 1):
        for way in range(2):
            @pl.when(gets(k, way))
            def _():
                b = s - 1 - k if way == 0 else s + 1 + k
                for j in range(m - 1):
                    across_in(1 + 2 * k + way, j, b).wait_recv()
                    across(1 + 2 * k + way, j, b).wait_send()

            @pl.when(sends(k, way))
            def _():
                along(k, way).wait_send()
    for k in range(1, n):
        p = lax.rem(s + n - k, n)
        remote(eo.at[p], eo.at[p], esend.at[k - 1], erecv.at[k - 1], {"sp": p}).wait_recv()
        part = wo.at[pl.ds(p * depth, depth)]
        remote(part, part, wsend.at[k - 1], wrecv.at[k - 1], {"sp": p}).wait_recv()
        extras[k - 1].wait_send()
        weights[k - 1].wait_send()
    for copy in (own_x, own_w, own_e):
        copy.wait()


def collect(n, m, x, w, e):
    rows, feats = x.shape
    vmem = pl.BlockSpec(memory_space=pltpu.VMEM)
    dma = pltpu.SemaphoreType.DMA
    hops = max(n - 1, 1)
    return pl.pallas_call(
        functools.partial(collect_kernel, n, m),
        out_shape=(
            jax.ShapeDtypeStruct((n * rows, m * feats), bf16),
            jax.ShapeDtypeStruct((n * w.shape[1], w.shape[2]), bf16),
            jax.ShapeDtypeStruct((n,) + e.shape, f32),
        ),
        in_specs=[vmem] * 3,
        out_specs=(vmem,) * 3,
        scratch_shapes=[
            dma((3,)),
            dma((2, hops)), dma((2, hops)),
            dma((2 * n - 1, max(m - 1, 1))), dma((2 * n - 1, max(m - 1, 1))),
            dma((hops,)), dma((hops,)), dma((hops,)), dma((hops,)),
        ],
        compiler_params=pltpu.CompilerParams(collective_id=0, has_side_effects=True),
    )(x, w, e)


def pick(ref, s, n, width):
    out = ref[:, :width]
    for i in range(1, n):
        out = jnp.where(s == i, ref[:, i * width : (i + 1) * width], out)
    return out


def mix_kernel(
    n, m, hc, cc, rows,
    x_ref, gain_ref, w_ref, e_ref, dd_ref, du_ref, db_ref, cd_ref, cu_ref, cb_ref, hs_ref, st_ref, taps_ref,
    mix_ref, conv_ref, sums_ref,
    proj, low, glu, maps, adds, qe, oi, states,
):
    s = lax.axis_index("sp")
    heads = hc // GROUP
    length = x_ref.shape[0]
    feats = x_ref.shape[1]
    block = 256 if length % 256 == 0 else rows

    @pl.loop(0, length // block)
    def _(i):
        at = pl.ds(pl.multiple_of(i * block, block), block)
        x = x_ref[at, :].astype(f32)
        normed = (x * lax.rsqrt(jnp.mean(x * x, axis=-1, keepdims=True) + 1e-06) * gain_ref[...]).astype(bf16)
        proj[at, :] = dot1(normed, w_ref[...])
        low[0, at, :] = jnp.tanh(dot1(normed, dd_ref[...])).astype(bf16)
        low[1, at, :] = dot1(normed, cd_ref[...]).astype(bf16)

    reach = taps_ref.shape[0] // 2
    top = 16 * ((reach + 15) // 16)
    glu[pl.ds(0, top), :] = jnp.zeros((top, cc), f32)
    glu[pl.ds(top + length, top), :] = jnp.zeros((top, cc), f32)
    base = 2 * hc
    gate = proj[:, base + cc : base + 2 * cc]
    glu[pl.ds(top, length), :] = (proj[:, base : base + cc] * jax.nn.sigmoid(gate)).astype(bf16).astype(f32)
    taps = pick(taps_ref, s, n, cc)
    step = 64
    for r in range(0, length, step):
        total = jnp.zeros((step, cc), f32)
        for j in range(taps_ref.shape[0]):
            total += taps[j : j + 1, :] * glu[pl.ds(r + top - reach + j, step), :]
        conv_ref[pl.ds(r, step), :] = total
    ones = jnp.ones((8, cc), f32)
    conv = conv_ref[...]
    row = lax.broadcasted_iota(jnp.int32, (8, length), 0)
    first = exact_rows(ones, conv)
    second = exact_rows(ones, conv * conv)
    sums_ref[...] = jnp.where(row == 0, first, jnp.where(row == 1, second, 0.0))

    size = 2 * CHUNK if rows % (2 * CHUNK) == 0 else CHUNK
    per = size // CHUNK
    ti = lax.broadcasted_iota(jnp.int32, (size, size), 0)
    tj = lax.broadcasted_iota(jnp.int32, (size, size), 1)
    same = ti // CHUNK == tj // CHUNK
    whole = same.astype(f32).astype(bf16)
    eye = (ti == tj).astype(f32)
    small_eye = (
        lax.broadcasted_iota(jnp.int32, (GROUP, GROUP), 0) == lax.broadcasted_iota(jnp.int32, (GROUP, GROUP), 1)
    ).astype(f32)
    du, cu = pick(du_ref, s, n, hc), pick(cu_ref, s, n, hc)
    db, cb = pick(db_ref, s, n, hc), pick(cb_ref, s, n, hc)
    hs = pick(hs_ref, s, n, hc)
    local_heads = e_ref.shape[1] // 2
    erow = lax.broadcasted_iota(jnp.int32, (2 * local_heads, GROUP), 0)

    for h in range(heads):
        lanes = slice(h * GROUP, (h + 1) * GROUP)
        klanes = slice(hc + h * GROUP, hc + (h + 1) * GROUP)
        vlanes = slice(base + 2 * cc + h * GROUP, base + 2 * cc + (h + 1) * GROUP)
        pick_offset = (erow == s * heads + h).astype(f32)
        pick_extra = (erow == local_heads + s * heads + h).astype(f32)

        @pl.loop(0, length // size)
        def _(i):
            at = pl.ds(pl.multiple_of(i * size, size), size)
            inner = rows // size
            if inner == 1:
                entry = e_ref[i]
            else:
                entry = e_ref[i // inner, :, pl.ds(pl.multiple_of((i % inner) * size, size), size)]
            offset = lax.dot_general(entry, pick_offset, TN, precision=lax.Precision.HIGHEST, preferred_element_type=f32)
            extra = lax.dot_general(entry, pick_extra, TN, precision=lax.Precision.HIGHEST, preferred_element_type=f32)
            pre = db[:, lanes] + dot1(low[0, at, :], du[:, lanes]) + offset
            lw = -jnp.exp(-jax.nn.softplus(-pre) - 0.5) + extra
            rate = jax.nn.sigmoid(cb[:, lanes] + dot1(low[1, at, :], cu[:, lanes]))
            q = proj[at, lanes].astype(bf16).astype(f32)
            k = proj[at, klanes].astype(bf16).astype(f32)
            vb = proj[at, vlanes].astype(bf16)
            unit = k * lax.rsqrt(jnp.sum(k * k, axis=-1, keepdims=True) + 1e-06)
            rated = unit * rate
            total = exact_left(whole, lw)
            for d in range(2):
                strict = same & ((ti > tj) if d == 0 else (ti < tj))
                upto = same & ((ti >= tj) if d == 0 else (ti <= tj))
                g = exact_left(upto.astype(f32).astype(bf16), lw)
                before = g - lw
                middle = 0.5 * total
                ahead = jnp.exp(middle - g)
                left = halves(jnp.concatenate([unit * jnp.exp(before - middle), q * jnp.exp(g - middle)], axis=0))
                right = halves(jnp.concatenate([rated * ahead, k * ahead], axis=0))
                scores = dot3(left, right, NT)
                a_ur = jnp.where(strict, scores[:size, :size], 0.0)
                a_uk = jnp.where(strict, scores[:size, size:], 0.0)
                a_qr = jnp.where(upto, scores[size:, :size], 0.0)
                a_qk = jnp.where(upto, scores[size:, size:], 0.0)
                width = 1
                inverse = eye - jnp.where((ti // 2 == tj // 2), a_ur, 0.0)
                width = 2
                while width < CHUNK:
                    part = jnp.where(
                        (ti // (2 * width) == tj // (2 * width)) & (ti // width != tj // width), a_ur, 0.0
                    )
                    pair = halves(inverse)
                    inverse = inverse - dot3(dot3(pair, part), pair)
                    width *= 2
                a_kv = halves(jnp.concatenate([a_uk, a_qk], axis=0))
                both = dot1(a_kv[0], vb) + dot1(a_kv[1], vb)
                wy = dot3(inverse, jnp.concatenate([unit * jnp.exp(before), both[:size]], axis=1))
                far = dot3(a_qr, wy)
                qe[d, at, :] = q * jnp.exp(g) - far[:, :GROUP]
                oi[d, at, :] = both[size:] - far[:, GROUP:]
                tail = jnp.exp(total - g)
                r_end, k_end = rated * tail, k * tail
                for c in range(per):
                    cut = slice(c * CHUNK, (c + 1) * CHUNK)
                    moved = dot3(wy[cut], r_end[cut], TN)
                    ke = halves(k_end[cut])
                    came = dot1(vb[cut], ke[0], TN) + dot1(vb[cut], ke[1], TN)
                    decay = jnp.exp(total[c * CHUNK : c * CHUNK + 1])
                    maps[d, i * per + c] = small_eye * decay - moved[:GROUP]
                    adds[d, i * per + c] = came - moved[GROUP:]

        chunks = length // CHUNK
        now = [st_ref[0, 0, s * heads + h], st_ref[0, 1, s * heads + h]]
        for c in range(chunks):
            for d in range(2):
                at = c if d == 0 else chunks - 1 - c
                states[d, at] = now[d]
                if c < chunks - 1:
                    now[d] = dot3(now[d], maps[d, at]) + adds[d, at]
        share = rows // m
        for c in range(chunks):
            cut = pl.ds(c * CHUNK, CHUNK)
            out = oi[0, cut, :] + oi[1, cut, :]
            for d in range(2):
                out += dot3(qe[d, cut, :], states[d, c], NT)
            centered = out - jnp.mean(out, axis=-1, keepdims=True)
            power = jnp.mean(centered * centered, axis=-1, keepdims=True)
            done = (centered * lax.rsqrt(power + 0.00064) * hs[:, lanes]).astype(bf16)
            for piece in range(0, CHUNK, min(share, CHUNK)):
                token = c * CHUNK + piece
                take = min(share, CHUNK)
                owner, inside = token // rows, token % rows
                mix_ref[inside // share, pl.ds(owner * share + inside % share, take), lanes] = done[piece : piece + take]


def exact_rows(ones, x):
    return lax.dot_general(ones, x, NT, precision=lax.Precision.HIGHEST, preferred_element_type=f32)


def mix(n, m, hc, cc, rows, *args):
    length = args[0].shape[0]
    vmem = pl.BlockSpec(memory_space=pltpu.VMEM)
    rank = args[4].shape[1]
    reach = args[12].shape[0] // 2
    top = 16 * ((reach + 15) // 16)
    chunks = length // CHUNK
    return pl.pallas_call(
        functools.partial(mix_kernel, n, m, hc, cc, rows),
        out_shape=(
            jax.ShapeDtypeStruct((m, length // m, hc), bf16),
            jax.ShapeDtypeStruct((length, cc), f32),
            jax.ShapeDtypeStruct((8, length), f32),
        ),
        in_specs=[vmem] * len(args),
        out_specs=(vmem,) * 3,
        scratch_shapes=[
            pltpu.VMEM((length, args[2].shape[1]), f32),
            pltpu.VMEM((2, length, rank), bf16),
            pltpu.VMEM((length + 2 * top, cc), f32),
            pltpu.VMEM((2, chunks, GROUP, GROUP), f32),
            pltpu.VMEM((2, chunks, GROUP, GROUP), f32),
            pltpu.VMEM((2, length, GROUP), f32),
            pltpu.VMEM((2, length, GROUP), f32),
            pltpu.VMEM((2, chunks, GROUP, GROUP), f32),
        ],
    )(*args)


def output_kernel(
    n, m, hc, cc, pack,
    mix_ref, conv_ref, sums_ref, cs_ref, wm_ref, wc_ref, out_ref,
    own, around, mates_act, sums_in, wm_in, wc_in, total, block,
    local, ssend, srecv, vsend, vrecv, asend, arecv, dsend, drecv, osend, orecv,
):
    s, t = lax.axis_index("sp"), lax.axis_index("tp")
    here = s * m + t
    everyone = n * m
    length = conv_ref.shape[0]
    half = length // m
    share = half // n
    columns = wm_ref.shape[1]
    packed = half // pack
    mates = [lax.rem(t + k, m) for k in range(1, m)]

    def other(k):
        p = lax.rem(here + k, everyone)
        return {"sp": p // m, "tp": p % m}

    greet([other(k) for k in range(1, everyone)])
    outs = []
    for k in range(1, everyone):
        outs.append(remote(sums_ref, sums_in.at[k - 1], ssend.at[k - 1], srecv.at[k - 1], other(k)))
    for j in range(m - 1):
        outs.append(remote(wm_ref, wm_in.at[j], vsend.at[0, j], vrecv.at[0, j], {"tp": mates[j]}))
        outs.append(remote(wc_ref, wc_in.at[j], vsend.at[1, j], vrecv.at[1, j], {"tp": mates[j]}))
    for copy in outs:
        copy.start()
    width = mix_ref.shape[2]
    for c in range(m):
        for i in range(pack):
            own[c, pl.ds(0, packed), pl.ds(i * hc, hc)] = mix_ref[c, pl.ds(i * packed, packed), :]
    for copy in outs[: everyone - 1]:
        copy.wait()
    stats = sums_ref[...]
    for k in range(everyone - 1):
        stats += sums_in[k]
    row = lax.broadcasted_iota(jnp.int32, (8, cc), 0)
    channels = cc * n * m

    def spread(which):
        return lax.dot_general(
            stats, (row == which).astype(f32), TN, precision=lax.Precision.HIGHEST, preferred_element_type=f32
        )

    mean = spread(0) / channels
    power = spread(1) / channels - mean * mean
    gain = pick(cs_ref, s, n, cc)
    done = jax.nn.silu((conv_ref[...] - mean) * lax.rsqrt(power + 1e-05) * gain).astype(bf16)
    for token in range(0, length, share):
        unit = token // share
        own[unit % m, pl.ds(packed + (unit // m) * share, share), :] = done[token : token + share]

    def along(k, way):
        b = s - k if way == 0 else s + k
        src = own if k == 0 else around.at[b]
        return remote(src, around.at[b], asend.at[way, k], arecv.at[way, k], {"sp": s + 1 if way == 0 else s - 1})

    def sends(k, way):
        return (s - k >= 0) & (s < n - 1) if way == 0 else (s + k < n) & (s > 0)

    def gets(k, way):
        return s - 1 - k >= 0 if way == 0 else s + 1 + k < n

    def across(index, j, b):
        src = own.at[mates[j]] if index == 0 else around.at[b, mates[j]]
        return remote(src, mates_act.at[j, b], dsend.at[index, j], drecv.at[index, j], {"tp": mates[j]})

    def add(b, act, wm, wc):
        w = wm[pl.ds(pl.multiple_of(b * hc, hc), hc), :]
        for i in range(pack):
            rows = pl.ds(i * packed, packed)
            total[rows, :] += dot1(act[pl.ds(0, packed), pl.ds(i * hc, hc)], w)
        total[...] += dot1(act[pl.ds(packed, half), :], wc[pl.ds(pl.multiple_of(b * cc, cc), cc), :])

    for way in range(2):
        @pl.when(sends(0, way))
        def _():
            along(0, way).start()
    for j in range(m - 1):
        across(0, j, s).start()
    total[...] = jnp.zeros_like(total)
    add(s, own.at[t], wm_ref, wc_ref)
    for copy in outs[everyone - 1 :]:
        copy.wait()

    def from_mates(index, b):
        for j in range(m - 1):
            across(index, j, b).wait_recv()
            add(b, mates_act.at[j, b], wm_in.at[j], wc_in.at[j])
            across(index, j, b).wait_send()

    for k in range(n - 1):
        for way in range(2):
            @pl.when(gets(k, way))
            def _():
                b = s - 1 - k if way == 0 else s + 1 + k
                remote(around.at[b], around.at[b], asend.at[way, k], arecv.at[way, k], {"sp": b}).wait_recv()
                if k + 1 < n - 1:
                    @pl.when(sends(k + 1, way))
                    def _():
                        along(k + 1, way).start()
                for j in range(m - 1):
                    across(1 + 2 * k + way, j, b).start()
                add(b, around.at[b, t], wm_ref, wc_ref)
        if k == 0:
            from_mates(0, s)
        else:
            for way in range(2):
                @pl.when(gets(k - 1, way))
                def _():
                    from_mates(2 * k - 1 + way, s - k if way == 0 else s + k)
    for way in range(2):
        @pl.when(gets(n - 2, way))
        def _():
            from_mates(2 * n - 3 + way, s - n + 1 if way == 0 else s + n - 1)
    for k in range(n - 1):
        for way in range(2):
            @pl.when(sends(k, way))
            def _():
                along(k, way).wait_send()
    block[...] = total[...].astype(bf16)
    mine = out_ref.at[:, pl.ds(pl.multiple_of(s * columns, columns), columns)]
    keep = pltpu.make_async_copy(block.at[pl.ds(s * share, share)], mine, local.at[0])
    keep.start()
    final = []
    for k in range(1, n):
        p = lax.rem(s + k, n)
        copy = remote(block.at[pl.ds(p * share, share)], mine, osend.at[k - 1], orecv.at[k - 1], {"sp": p})
        copy.start()
        final.append(copy)
    for k in range(1, n):
        p = lax.rem(s + n - k, n)
        part = out_ref.at[:, pl.ds(pl.multiple_of(p * columns, columns), columns)]
        remote(part, part, osend.at[k - 1], orecv.at[k - 1], {"sp": p}).wait_recv()
        final[k - 1].wait_send()
    keep.wait()


def output(n, m, hc, cc, mixed, conv, sums, cs, wm, wc):
    length = conv.shape[0]
    half, columns = length // m, wm.shape[1]
    pack = max(cc // hc, 1)
    rows = half // pack + half
    vmem = pl.BlockSpec(memory_space=pltpu.VMEM)
    dma = pltpu.SemaphoreType.DMA
    hops, mates = max(n - 1, 1), max(m - 1, 1)
    return pl.pallas_call(
        functools.partial(output_kernel, n, m, hc, cc, pack),
        out_shape=jax.ShapeDtypeStruct((half // n, n * columns), bf16),
        in_specs=[vmem] * 6,
        out_specs=vmem,
        scratch_shapes=[
            pltpu.VMEM((m, rows, cc), bf16),
            pltpu.VMEM((n, m, rows, cc), bf16),
            pltpu.VMEM((mates, n, rows, cc), bf16),
            pltpu.VMEM((n * m - 1, 8, length), f32),
            pltpu.VMEM((mates,) + wm.shape, bf16),
            pltpu.VMEM((mates,) + wc.shape, bf16),
            pltpu.VMEM((half, columns), f32),
            pltpu.VMEM((half, columns), bf16),
            dma((1,)),
            dma((n * m - 1,)), dma((n * m - 1,)),
            dma((2, mates)), dma((2, mates)),
            dma((2, hops)), dma((2, hops)),
            dma((2 * n - 1, mates)), dma((2 * n - 1, mates)),
            dma((hops,)), dma((hops,)),
        ],
        compiler_params=pltpu.CompilerParams(collective_id=1, has_side_effects=True),
    )(mixed, conv, sums, cs, wm, wc)


highest = lax.Precision.HIGHEST


def carried_in(x, axis, combine, identity, reverse):
    length, here = (lax.axis_size(axis), lax.axis_index(axis))
    everything = jax.tree.map(
        lambda part, kind: lax.all_gather(part.astype(kind), axis), x, (jnp.bfloat16, jnp.bfloat16)
    )
    start = jax.tree.map(
        lambda part, zero: jnp.broadcast_to(jnp.asarray(zero, part.dtype), part.shape), x, identity
    )

    def hop(k, before):
        at = length - 1 - k if reverse else k
        reached = at > here if reverse else at < here
        new = combine(
            before, jax.tree.map(lambda part, own: part[at].astype(own.dtype), everything, x)
        )
        return jax.tree.map(lambda a, b: jnp.where(reached, a, b), new, before)

    return lax.fori_loop(0, length, hop, start)


def padded_2(block, sides, width):
    for axis, dim in sides:
        count = lax.axis_size(axis)
        forward = [(i, i + 1) for i in range(count - 1)]
        backward = [(target, source) for source, target in forward]
        low = lax.ppermute(
            lax.slice_in_dim(block, block.shape[dim] - width, None, axis=dim), axis, forward
        )
        high = lax.ppermute(lax.slice_in_dim(block, 0, width, axis=dim), axis, backward)
        block = jnp.concatenate([low, block, high], axis=dim)
    return block


def split_heads(values):
    return values.reshape(values.shape[0], -1, GROUP)


def paired(values):
    return jnp.stack([values, jnp.flip(values, 0)], 1)


def local_step(stacked, inputs):
    fading_multiplier, unit_key, rated_key, keys, values, query = inputs
    projected = jnp.einsum("dhvk,dhk->dhv", stacked, unit_key, precision=highest)
    outer = values[..., None] * keys[:, :, None, :]
    added = jnp.concatenate([jnp.zeros_like(outer), outer], axis=2)
    stacked = (
        stacked * fading_multiplier[:, :, None, :]
        - projected[..., None] * rated_key[:, :, None, :]
        + added
    )
    return (stacked, jnp.einsum("dhvk,dhk->dhv", stacked, query, precision=highest))


def chain_pair(earlier, later):
    product = jnp.einsum("hij,hjk->hik", earlier[0], later[0], precision=highest)
    moved = jnp.einsum("hij,hjk->hik", earlier[1], later[0], precision=highest) + later[1]
    return (product, moved)


def carry_in(initial_memory_matrix, prefix):
    return (
        jnp.einsum("hij,hjk->hik", initial_memory_matrix, prefix[0], precision=highest) + prefix[1]
    )


def head_norm(summed, head_norm_scale):
    centered = summed - jnp.mean(summed, axis=-1, keepdims=True)
    scaled = centered * lax.rsqrt(jnp.mean(centered * centered, axis=-1, keepdims=True) + 0.00064)
    return (
        (scaled * head_norm_scale.reshape(-1, GROUP))
        .reshape(summed.shape[0], -1)
        .astype(jnp.bfloat16)
    )


def rounded(total):
    return lax.optimization_barrier(total.astype(jnp.bfloat16)).astype(jnp.float32)


def mixer_branch(
    normed,
    sums,
    decay_down_weight,
    decay_up_weight,
    decay_bias_base,
    decay_position_offset,
    extra_log_decay,
    correction_down_weight,
    correction_up_weight,
    correction_rate_bias,
    head_norm_scale,
    starting_states,
):
    query = rounded(sums[0])
    keys = rounded(sums[1])
    values = rounded(sums[2])
    low_decay = jnp.tanh(
        jnp.dot(normed, decay_down_weight, preferred_element_type=jnp.float32)
    ).astype(jnp.bfloat16)
    fading_raw_scores = (
        decay_bias_base
        + jnp.dot(low_decay, decay_up_weight, preferred_element_type=jnp.float32)
        + jnp.repeat(decay_position_offset[0], GROUP, axis=1)
    )
    fading_multiplier = jnp.exp(
        -jnp.exp(-jax.nn.softplus(-fading_raw_scores) - 0.5)
        + jnp.repeat(extra_log_decay[0], GROUP, axis=1)
    )
    low_rate = jnp.dot(normed, correction_down_weight, preferred_element_type=jnp.float32).astype(
        jnp.bfloat16
    )
    rate = jax.nn.sigmoid(
        correction_rate_bias
        + jnp.dot(low_rate, correction_up_weight, preferred_element_type=jnp.float32)
    )
    key_heads = split_heads(keys)
    unit_key = key_heads * lax.rsqrt(jnp.sum(key_heads * key_heads, axis=-1, keepdims=True) + 1e-06)
    rated_key = unit_key * split_heads(rate)
    steps = tuple(
        (
            paired(item)
            for item in (
                split_heads(fading_multiplier),
                unit_key,
                rated_key,
                key_heads,
                split_heads(values),
                split_heads(query),
            )
        )
    )
    heads_here = key_heads.shape[1]
    identity = jnp.broadcast_to(
        jnp.eye(GROUP, dtype=jnp.float32),
        (2, heads_here, GROUP, GROUP),
    )
    nothing = jnp.zeros((2, heads_here, GROUP, GROUP), jnp.float32)
    start = jnp.concatenate([identity, nothing], axis=2)
    ends, emitted = lax.scan(local_step, start, steps, unroll=8)
    transfer = ends[:, :, :GROUP]
    alone = ends[:, :, GROUP:]
    through = emitted[..., :GROUP]
    own_part = emitted[..., GROUP:]
    before = carried_in((transfer[0], alone[0]), "sp", chain_pair, (identity[0], nothing[0]), False)
    after = carried_in((transfer[1], alone[1]), "sp", chain_pair, (identity[1], nothing[1]), True)
    starts = jnp.stack(
        [carry_in(starting_states[0, 0], before), carry_in(starting_states[0, 1], after)], 0
    )
    outputs = jnp.einsum("dhvk,tdhk->tdhv", starts, through, precision=highest) + own_part
    summed = outputs[:, 0] + jnp.flip(outputs[:, 1], 0)
    return head_norm(summed, head_norm_scale)


def conv_branch(sums, depthwise_taps_weight, channel_norm_scale):
    glu = (sums[0] * jax.nn.sigmoid(sums[1])).astype(jnp.bfloat16)
    reach = depthwise_taps_weight.shape[0] // 2
    padded = padded_2(glu, (("sp", 0),), reach)
    conv = lax.conv_general_dilated(
        padded.astype(jnp.float32)[None],
        depthwise_taps_weight[:, None, :],
        (1,),
        "VALID",
        dimension_numbers=("NWC", "WIO", "NWC"),
        feature_group_count=depthwise_taps_weight.shape[1],
        precision=highest,
    )[0]
    first, second = lax.psum((jnp.sum(conv, axis=-1), jnp.sum(conv * conv, axis=-1)), "tp")
    width = conv.shape[1] * lax.axis_size("tp")
    mean = first / width
    power = second / width - mean * mean
    return jax.nn.silu(
        (conv - mean[:, None]) * lax.rsqrt(power[:, None] + 1e-05) * channel_norm_scale
    ).astype(jnp.bfloat16)


def spread_device(
    inputs,
    input_norm_scale,
    query_matrix,
    key_matrix,
    value_matrix,
    decay_down_weight,
    decay_up_weight,
    decay_bias_base,
    decay_position_offset,
    extra_log_decay,
    correction_down_weight,
    correction_up_weight,
    correction_rate_bias,
    head_norm_scale,
    starting_states,
    pointwise_value_weight,
    pointwise_gate_weight,
    depthwise_taps_weight,
    channel_norm_scale,
    mixer_output_weight,
    convolution_output_weight,
):
    symbol_vectors = lax.all_gather(inputs[0], "tp", axis=1, tiled=True)
    as_float = symbol_vectors.astype(jnp.float32)
    normed = (
        as_float
        * lax.rsqrt(jnp.mean(as_float * as_float, axis=-1, keepdims=True) + 1e-06)
        * input_norm_scale
    ).astype(jnp.bfloat16)
    mixer_args = (
        decay_down_weight,
        decay_up_weight,
        decay_bias_base,
        decay_position_offset,
        extra_log_decay,
        correction_down_weight,
        correction_up_weight,
        correction_rate_bias,
        head_norm_scale,
        starting_states,
    )
    pieces = (
        lax.all_gather(query_matrix, "sp", axis=0, tiled=True),
        lax.all_gather(key_matrix, "sp", axis=0, tiled=True),
        lax.all_gather(value_matrix, "sp", axis=0, tiled=True),
        lax.all_gather(pointwise_value_weight, "sp", axis=0, tiled=True),
        lax.all_gather(pointwise_gate_weight, "sp", axis=0, tiled=True),
    )
    sums = tuple((jnp.dot(normed, piece, preferred_element_type=jnp.float32) for piece in pieces))
    mixer_out = mixer_branch(normed, sums[:3], *mixer_args)
    conv_out = conv_branch(sums[3:], depthwise_taps_weight, channel_norm_scale)
    joined = jnp.concatenate([mixer_out, conv_out], axis=1)
    weight_rows = jnp.concatenate([mixer_output_weight, convolution_output_weight], axis=0)
    columns = lax.all_gather(weight_rows, "sp", axis=1, tiled=True)
    moved = lax.all_to_all(joined, "tp", split_axis=0, concat_axis=1, tiled=True)
    every_row = lax.all_gather(columns, "tp", axis=0, tiled=True)
    total = jnp.dot(moved, every_row, preferred_element_type=jnp.float32)
    return total.astype(jnp.bfloat16)[None]


def per_device(
    inputs, input_norm_scale, query_matrix, key_matrix, value_matrix,
    decay_down_weight, decay_up_weight, decay_bias_base, decay_position_offset, extra_log_decay,
    correction_down_weight, correction_up_weight, correction_rate_bias, head_norm_scale, starting_states,
    pointwise_value_weight, pointwise_gate_weight, depthwise_taps_weight, channel_norm_scale,
    mixer_output_weight, convolution_output_weight,
):
    n, m = lax.axis_size("sp"), lax.axis_size("tp")
    if query_matrix.shape[1] % (n * GROUP) or pointwise_value_weight.shape[1] % (n * 128):
        return spread_device(
            inputs, input_norm_scale, query_matrix, key_matrix, value_matrix,
            decay_down_weight, decay_up_weight, decay_bias_base, decay_position_offset, extra_log_decay,
            correction_down_weight, correction_up_weight, correction_rate_bias, head_norm_scale, starting_states,
            pointwise_value_weight, pointwise_gate_weight, depthwise_taps_weight, channel_norm_scale,
            mixer_output_weight, convolution_output_weight,
        )
    x = inputs[0]
    rows = x.shape[0]
    depth = query_matrix.shape[0]
    hc, cc = query_matrix.shape[1] // n, pointwise_value_weight.shape[1] // n
    parts = [query_matrix, key_matrix, pointwise_value_weight, pointwise_gate_weight, value_matrix]
    w = jnp.concatenate([part.reshape(depth, n, -1) for part in parts], axis=2).transpose(1, 0, 2)
    e = jnp.concatenate([decay_position_offset[0], extra_log_decay[0]], axis=1).T
    everything, columns, shifts = collect(n, m, x, w, e)
    mixed, conv, sums = mix(
        n, m, hc, cc, rows,
        everything, input_norm_scale[None], columns, shifts,
        decay_down_weight, decay_up_weight, decay_bias_base[None],
        correction_down_weight, correction_up_weight, correction_rate_bias[None],
        head_norm_scale[None], starting_states, depthwise_taps_weight,
    )
    return output(
        n, m, hc, cc, mixed, conv, sums, channel_norm_scale[None], mixer_output_weight, convolution_output_weight
    )[None]


def solution(mesh):
    return jax.shard_map(
        per_device,
        mesh=mesh,
        in_specs=(
            P("fs", "sp", "tp"),
            P(),
            P("sp", "tp"),
            P("sp", "tp"),
            P("sp", "tp"),
            P(),
            P(None, "tp"),
            P("tp"),
            P("fs", "sp", "tp"),
            P("fs", "sp", "tp"),
            P(),
            P(None, "tp"),
            P("tp"),
            P("tp"),
            P("fs", None, "tp", None, None),
            P("sp", "tp"),
            P("sp", "tp"),
            P(None, "tp"),
            P("tp"),
            P("tp", "sp"),
            P("tp", "sp"),
        ),
        out_specs=P("fs", ("sp", "tp"), None),
        check_vma=False,
    )
```

profile of v0, /device:TPU:0, one launch (start us, length us, event | category | flops | bytes accessed | tf_op | source)
XLA Modules:
  0.0 152.9 jit_solution(7599009950767042130)
XLA Ops:
  0.0 0.0 copy-start
  0.0 0.0 copy-start.2
  0.0 1.4 maximum_bitcast_fusion.e_ref
  1.4 1.1 copy.22
  2.5 0.3 copy.27
  2.7 1.1 copy.23
  3.9 0.0 copy-start.1
  3.9 0.3 copy.28
  4.1 0.0 copy-done.2
  4.2 0.1 copy.26
  4.3 0.3 copy.31
  4.6 0.0 copy-done
  4.6 0.2 copy.24
  4.8 0.3 copy.29
  5.1 0.0 copy-done.1
  5.1 0.2 copy.25
  5.3 0.3 copy.30
  5.6 4.1 %concatenate.6 = bf16[512,4,448]{2,0,1:T(8,128)(2,1)} concatenate(bf16[512,4,64]{2,0,1:T(8,128)(2,1)S(1)} %copy.27, bf16[512,4,64]{2,0,1:T(8,128)(2,1)S(1)} %copy.28, bf16[512,4,128]{2,0,1:T(8,128)(2,1)S(1)} %copy.29, bf16[512,4,128]{2,0,1:T(8,128)(2,1)S(1)} %copy.30, bf16[512,4,64]{2,0,1:T(8,128)(2,1)S(1)} %copy.31), dimensions={2} | concatenate | bytes 3670016 | tf_op jit(solution)/shard_map/concatenate | solution.py:793
  9.7 73.8 %shard_map.199 = (bf16[512,2048]{1,0:T(8,128)(2,1)}, bf16[2048,448]{1,0:T(8,128)(2,1)}, f32[4,8,128]{2,1,0:T(8,128)}) custom-call(bf16[128,1024]{1,0:T(8,128)(2,1)} %bitcast.24, bf16[4,512,448]{2,1,0:T(8,128)(2,1)} %bitcast.17, f32[8,128]{1,0:T(8,128)} %maximum_bitcast_fusion.e_ref), custom_call_target="tpu_custom_call" | custom-call | tf_op jit(solution)/shard_map/pallas_call | solution.py:151
  83.5 32.2 %shard_map.200 = (bf16[2,256,64]{2,1,0:T(8,128)(2,1)}, f32[512,128]{1,0:T(8,128)}, f32[8,512]{1,0:T(8,128)}) custom-call(bf16[512,2048]{1,0:T(8,128)(2,1)} %get-tuple-element.11.x_ref, f32[1,2048]{1,0:T(1,128)} %bitcast.25, bf16[2048,448]{1,0:T(8,128)(2,1)} %get-tuple-element.12.w_ref, f32[4,8,128]{2,1,0:T(8,128)} %get-tuple-element.13.e_ref, ...), custom_call_target="tpu_custom_call" | custom-call | tf_op jit(solution)/shard_map/pallas_call | solution.py:337
  115.7 35.5 %shard_map.201 = bf16[64,2048]{1,0:T(8,128)(2,1)} custom-call(bf16[2,256,64]{2,1,0:T(8,128)(2,1)} %get-tuple-element.14.mix_ref, f32[512,128]{1,0:T(8,128)} %get-tuple-element.15.conv_ref, f32[8,512]{1,0:T(8,128)} %get-tuple-element.16.sums_ref, f32[1,512]{1,0:T(1,128)} %bitcast.26, bf16[256,512]{1,0:T(8,128)(2,1)} %wm_ref.1, bf16[512,512]{1,0:T(8,128)(2,1)} %wc_ref.1), custom_call_target="tpu_custom_call" | custom-call | tf_op jit(solution)/shard_map/pallas_call | solution.py:507
  151.2 1.7 %copy.33 = bf16[1,64,2048]{2,1,0:T(8,128)(2,1)} copy(bf16[1,64,2048]{2,1,0:T(8,128)(2,1)} %bitcast.23) | data formatting | bytes 524288
Async XLA Ops:
  0.0 4.6 %copy-start = (bf16[512,512]{1,0:T(8,128)(2,1)S(1)}, bf16[512,512]{1,0:T(8,128)(2,1)}, u32[]{:S(2)}) copy-start(bf16[512,512]{1,0:T(8,128)(2,1)} %param.36) | copy-start | bytes 1572868
  0.0 4.1 %copy-start.2 = (bf16[512,256]{1,0:T(8,128)(2,1)S(1)}, bf16[512,256]{1,0:T(8,128)(2,1)}, u32[]{:S(2)}) copy-start(bf16[512,256]{1,0:T(8,128)(2,1)} %param.25) | copy-start | bytes 786436
  3.9 1.2 copy-start.1
where the time goes:
time: 153 us
  Pallas kernels  141 us (92%)
  local copies, waits for them, and re-layouts  9.9 us (6%)
    pallas_call x1, Pallas kernels, collect(): pl.pallas_call(functools.partial(collect_kernel, n, m), out_shape=(jax.Sh...  73.8 us
    pallas_call x1, Pallas kernels, output(): pl.pallas_call(functools.partial(output_kernel, n, m, hc, cc, pack), out_...  35.5 us
    pallas_call x1, Pallas kernels, mix(): pl.pallas_call(functools.partial(mix_kernel, n, m, hc, cc, rows), out_sha...  32.2 us
    unnamed x12, local copies, waits for them, and re-layouts  4.43 us
    concatenate x1, local copies, waits for them, and re-layouts, per_device(): jnp.concatenate([part.reshape(depth, n, -1) for part in parts], axis=2)  4.11 us

commit v1 on v0

--- a/solution.py
+++ b/solution.py
@@ -50,27 +50,53 @@
     pl.semaphore_wait(barrier, len(peers))
 
 
-def collect_kernel(n, m, x_ref, w_ref, e_ref, xo, wo, eo, local, xsend, xrecv, dsend, drecv, wsend, wrecv, esend, erecv):
-    s, t = lax.axis_index("sp"), lax.axis_index("tp")
+def pick_lanes(ref, p, width):
+    return ref[:, p * width : (p + 1) * width]
+
+
+def collect_kernel(
+    n, m, nf, cut,
+    x_ref, q_ref, k_ref, pv_ref, pg_ref, v_ref, e_ref, xo, wo, eo, ready,
+    local, xsend, xrecv, dsend, drecv, wsend, wrecv, fsend, frecv, esend, erecv,
+):
+    s, t, f = lax.axis_index("sp"), lax.axis_index("tp"), lax.axis_index("fs")
     rows, feats = x_ref.shape
-    depth = w_ref.shape[1]
-
-    def slot(b, c):
-        return xo.at[pl.ds(b * rows, rows), pl.ds(pl.multiple_of(c * feats, feats), feats)]
-
-    own_x = pltpu.make_async_copy(x_ref, slot(s, t), local.at[0])
-    own_w = pltpu.make_async_copy(w_ref.at[s], wo.at[pl.ds(s * depth, depth)], local.at[1])
-    own_e = pltpu.make_async_copy(e_ref, eo.at[s], local.at[2])
-    for copy in (own_x, own_w, own_e):
-        copy.start()
+    depth = q_ref.shape[0]
+    quarter = depth // nf
+    some = rows // cut
+
+    def slot(b, c, i):
+        return xo.at[pl.ds(b * rows + i * some, some), pl.ds(pl.multiple_of(c * feats, feats), feats)]
+
+    def piece(p, g):
+        return wo.at[pl.ds(p * depth + g * quarter, quarter)]
+
     ring = [lax.rem(s + k, n) for k in range(1, n)]
     mates = [lax.rem(t + k, m) for k in range(1, m)]
-    greet([{"sp": p} for p in ring] + [{"tp": c} for c in mates])
-
-    def along(k, way):
+    planes = [lax.rem(f + k, nf) for k in range(1, nf)]
+    barrier = pltpu.get_barrier_semaphore()
+    peers = [{"sp": p} for p in ring] + [{"tp": c} for c in mates] + [{"fs": g} for g in planes]
+    for where in peers:
+        pl.semaphore_signal(barrier, inc=1, device_id=where, device_id_type=MESH)
+    own_x = pltpu.make_async_copy(
+        x_ref, xo.at[pl.ds(s * rows, rows), pl.ds(pl.multiple_of(t * feats, feats), feats)], local.at[0]
+    )
+    own_e = pltpu.make_async_copy(e_ref, eo.at[s], local.at[2])
+    own_x.start()
+    own_e.start()
+    for p in range(n):
+        ready[p] = jnp.concatenate(
+            [pick_lanes(ref, p, ref.shape[1] // n) for ref in (q_ref, k_ref, pv_ref, pg_ref, v_ref)], axis=1
+        )
+    own_w = pltpu.make_async_copy(ready.at[s], wo.at[pl.ds(s * depth, depth)], local.at[1])
+    pl.semaphore_wait(barrier, len(peers))
+
+    def along(k, way, i):
         b = s - k if way == 0 else s + k
-        src = x_ref if k == 0 else slot(b, t)
-        return remote(src, slot(b, t), xsend.at[way, k], xrecv.at[way, k], {"sp": s + 1 if way == 0 else s - 1})
+        src = x_ref.at[pl.ds(i * some, some)] if k == 0 else slot(b, t, i)
+        return remote(
+            src, slot(b, t, i), xsend.at[way, k, i], xrecv.at[way, k, i], {"sp": s + 1 if way == 0 else s - 1}
+        )
 
     def sends(k, way):
         return (s - k >= 0) & (s < n - 1) if way == 0 else (s + k < n) & (s > 0)
@@ -78,93 +104,114 @@
     def gets(k, way):
         return s - 1 - k >= 0 if way == 0 else s + 1 + k < n
 
-    def across(index, j, b):
-        src = x_ref if index == 0 else slot(b, t)
-        return remote(src, slot(b, t), dsend.at[index, j], drecv.at[index, j], {"tp": mates[j]})
-
-    def across_in(index, j, b):
+    def across(index, j, b, i):
+        src = x_ref.at[pl.ds(i * some, some)] if index == 0 else slot(b, t, i)
+        return remote(src, slot(b, t, i), dsend.at[index, j, i], drecv.at[index, j, i], {"tp": mates[j]})
+
+    def across_in(index, j, b, i):
         c = lax.rem(t + m - 1 - j, m)
-        return remote(slot(b, c), slot(b, c), dsend.at[index, j], drecv.at[index, j], {"tp": mates[j]})
-
-    for way in range(2):
-        @pl.when(sends(0, way))
-        def _():
-            along(0, way).start()
-    extras = []
-    for k in range(1, n):
-        copy = remote(e_ref, eo.at[s], esend.at[k - 1], erecv.at[k - 1], {"sp": ring[k - 1]})
-        copy.start()
-        extras.append(copy)
-    weights = []
+        return remote(slot(b, c, i), slot(b, c, i), dsend.at[index, j, i], drecv.at[index, j, i], {"tp": mates[j]})
+
+    started = []
     for k in range(1, n):
         p = ring[k - 1]
-        copy = remote(
-            w_ref.at[p], wo.at[pl.ds(s * depth, depth)], wsend.at[k - 1], wrecv.at[k - 1], {"sp": p}
+        started.append(
+            remote(
+                ready.at[p, pl.ds(f * quarter, quarter)], piece(s, f), wsend.at[k - 1], wrecv.at[k - 1], {"sp": p}
+            )
         )
+        started.append(remote(e_ref, eo.at[s], esend.at[k - 1], erecv.at[k - 1], {"sp": p}))
+    for copy in started:
         copy.start()
-        weights.append(copy)
-    for j in range(m - 1):
-        across(0, j, s).start()
+    for i in range(cut):
+        for way in range(2):
+            @pl.when(sends(0, way))
+            def _():
+                along(0, way, i).start()
+    for i in range(cut):
+        for j in range(m - 1):
+            across(0, j, s, i).start()
+    own_w.start()
+    for k in range(1, n):
+        p = lax.rem(s + n - k, n)
+        remote(piece(p, f), piece(p, f), wsend.at[k - 1], wrecv.at[k - 1], {"sp": p}).wait_recv()
+        for g in range(nf - 1):
+            copy = remote(piece(p, f), piece(p, f), fsend.at[k - 1, g], frecv.at[k - 1, g], {"fs": planes[g]})
+            copy.start()
+            started.append(copy)
+    for k in range(n - 1):
+        for i in range(cut):
+            for way in range(2):
+                @pl.when(gets(k, way))
+                def _():
+                    b = s - 1 - k if way == 0 else s + 1 + k
+                    remote(
+                        slot(b, t, i), slot(b, t, i), xsend.at[way, k, i], xrecv.at[way, k, i], {"sp": b}
+                    ).wait_recv()
+                    if k + 1 < n - 1:
+                        @pl.when(sends(k + 1, way))
+                        def _():
+                            along(k + 1, way, i).start()
+                    for j in range(m - 1):
+                        across(1 + 2 * k + way, j, b, i).start()
+    for i in range(cut):
+        for j in range(m - 1):
+            across_in(0, j, s, i).wait_recv()
+            across(0, j, s, i).wait_send()
     for k in range(n - 1):
         for way in range(2):
             @pl.when(gets(k, way))
             def _():
                 b = s - 1 - k if way == 0 else s + 1 + k
-                remote(slot(b, t), slot(b, t), xsend.at[way, k], xrecv.at[way, k], {"sp": b}).wait_recv()
-                if k + 1 < n - 1:
-                    @pl.when(sends(k + 1, way))
-                    def _():
-                        along(k + 1, way).start()
-                for j in range(m - 1):
-                    across(1 + 2 * k + way, j, b).start()
-    for j in range(m - 1):
-        across_in(0, j, s).wait_recv()
-        across(0, j, s).wait_send()
-    for k in range(n - 1):
-        for way in range(2):
-            @pl.when(gets(k, way))
-            def _():
-                b = s - 1 - k if way == 0 else s + 1 + k
-                for j in range(m - 1):
-                    across_in(1 + 2 * k + way, j, b).wait_recv()
-                    across(1 + 2 * k + way, j, b).wait_send()
+                for i in range(cut):
+                    for j in range(m - 1):
+                        across_in(1 + 2 * k + way, j, b, i).wait_recv()
+                        across(1 + 2 * k + way, j, b, i).wait_send()
 
             @pl.when(sends(k, way))
             def _():
-                along(k, way).wait_send()
+                for i in range(cut):
+                    along(k, way, i).wait_send()
     for k in range(1, n):
         p = lax.rem(s + n - k, n)
         remote(eo.at[p], eo.at[p], esend.at[k - 1], erecv.at[k - 1], {"sp": p}).wait_recv()
-        part = wo.at[pl.ds(p * depth, depth)]
-        remote(part, part, wsend.at[k - 1], wrecv.at[k - 1], {"sp": p}).wait_recv()
-        extras[k - 1].wait_send()
-        weights[k - 1].wait_send()
+        for g in range(nf - 1):
+            source = lax.rem(f + nf - 1 - g, nf)
+            remote(
+                piece(p, source), piece(p, source), fsend.at[k - 1, g], frecv.at[k - 1, g], {"fs": source}
+            ).wait_recv()
+    for copy in started:
+        copy.wait_send()
     for copy in (own_x, own_w, own_e):
         copy.wait()
 
 
-def collect(n, m, x, w, e):
+def collect(n, m, nf, x, parts, e):
     rows, feats = x.shape
     vmem = pl.BlockSpec(memory_space=pltpu.VMEM)
     dma = pltpu.SemaphoreType.DMA
-    hops = max(n - 1, 1)
+    hops, mates, planes, cut = max(n - 1, 1), max(m - 1, 1), max(nf - 1, 1), 2
+    depth, wide = parts[0].shape[0], sum(part.shape[1] for part in parts) // n
     return pl.pallas_call(
-        functools.partial(collect_kernel, n, m),
+        functools.partial(collect_kernel, n, m, nf, cut),
         out_shape=(
             jax.ShapeDtypeStruct((n * rows, m * feats), bf16),
-            jax.ShapeDtypeStruct((n * w.shape[1], w.shape[2]), bf16),
+            jax.ShapeDtypeStruct((n * depth, wide), bf16),
             jax.ShapeDtypeStruct((n,) + e.shape, f32),
         ),
-        in_specs=[vmem] * 3,
+        in_specs=[vmem] * 7,
         out_specs=(vmem,) * 3,
         scratch_shapes=[
+            pltpu.VMEM((n, depth, wide), bf16),
             dma((3,)),
-            dma((2, hops)), dma((2, hops)),
-            dma((2 * n - 1, max(m - 1, 1))), dma((2 * n - 1, max(m - 1, 1))),
-            dma((hops,)), dma((hops,)), dma((hops,)), dma((hops,)),
+            dma((2, hops, cut)), dma((2, hops, cut)),
+            dma((2 * n - 1, mates, cut)), dma((2 * n - 1, mates, cut)),
+            dma((hops,)), dma((hops,)),
+            dma((hops, planes)), dma((hops, planes)),
+            dma((hops,)), dma((hops,)),
         ],
         compiler_params=pltpu.CompilerParams(collective_id=0, has_side_effects=True),
-    )(x, w, e)
+    )(x, *parts, e)
 
 
 def pick(ref, s, n, width):
@@ -389,6 +436,64 @@
     for c in range(m):
         for i in range(pack):
             own[c, pl.ds(0, packed), pl.ds(i * hc, hc)] = mix_ref[c, pl.ds(i * packed, packed), :]
+    pieces = m + 1
+
+    def slab(ref, i):
+        if i == 0:
+            return ref.at[:, pl.ds(0, packed)]
+        return ref.at[lax.rem(t + i, m), pl.ds(packed, half)]
+
+    def along(k, way, i):
+        b = s - k if way == 0 else s + k
+        src = slab(own if k == 0 else around.at[b], i)
+        return remote(
+            src, slab(around.at[b], i), asend.at[way, k, i], arecv.at[way, k, i], {"sp": s + 1 if way == 0 else s - 1}
+        )
+
+    def sends(k, way):
+        return (s - k >= 0) & (s < n - 1) if way == 0 else (s + k < n) & (s > 0)
+
+    def gets(k, way):
+        return s - 1 - k >= 0 if way == 0 else s + 1 + k < n
+
+    def across(index, j, b, i):
+        at = pl.ds(0, packed) if i == 0 else pl.ds(packed, half)
+        src = own.at[mates[j], at] if index == 0 else around.at[b, mates[j], at]
+        return remote(src, mates_act.at[j, b, at], dsend.at[index, j, i], drecv.at[index, j, i], {"tp": mates[j]})
+
+    def add(b, act, wm, wc):
+        w = wm[pl.ds(pl.multiple_of(b * hc, hc), hc), :]
+        for i in range(pack):
+            rows = pl.ds(i * packed, packed)
+            total[rows, :] += dot1(act[pl.ds(0, packed), pl.ds(i * hc, hc)], w)
+        total[...] += dot1(act[pl.ds(packed, half), :], wc[pl.ds(pl.multiple_of(b * cc, cc), cc), :])
+
+    def pass_on(k, i):
+        for way in range(2):
+            @pl.when(gets(k, way))
+            def _():
+                b = s - 1 - k if way == 0 else s + 1 + k
+                part = slab(around.at[b], i)
+                remote(part, part, asend.at[way, k, i], arecv.at[way, k, i], {"sp": b}).wait_recv()
+                if k + 1 < n - 1:
+                    @pl.when(sends(k + 1, way))
+                    def _():
+                        along(k + 1, way, i).start()
+                if i == 0:
+                    for j in range(m - 1):
+                        across(1 + 2 * k + way, j, b, 0).start()
+                elif i < m:
+                    across(1 + 2 * k + way, i - 1, b, 1).start()
+
+    def begin(i):
+        for way in range(2):
+            @pl.when(sends(0, way))
+            def _():
+                along(0, way, i).start()
+
+    begin(0)
+    for j in range(m - 1):
+        across(0, j, s, 0).start()
     for copy in outs[: everyone - 1]:
         copy.wait()
     stats = sums_ref[...]
@@ -410,57 +515,33 @@
         unit = token // share
         own[unit % m, pl.ds(packed + (unit // m) * share, share), :] = done[token : token + share]
 
-    def along(k, way):
-        b = s - k if way == 0 else s + k
-        src = own if k == 0 else around.at[b]
-        return remote(src, around.at[b], asend.at[way, k], arecv.at[way, k], {"sp": s + 1 if way == 0 else s - 1})
-
-    def sends(k, way):
-        return (s - k >= 0) & (s < n - 1) if way == 0 else (s + k < n) & (s > 0)
-
-    def gets(k, way):
-        return s - 1 - k >= 0 if way == 0 else s + 1 + k < n
-
-    def across(index, j, b):
-        src = own.at[mates[j]] if index == 0 else around.at[b, mates[j]]
-        return remote(src, mates_act.at[j, b], dsend.at[index, j], drecv.at[index, j], {"tp": mates[j]})
-
-    def add(b, act, wm, wc):
-        w = wm[pl.ds(pl.multiple_of(b * hc, hc), hc), :]
-        for i in range(pack):
-            rows = pl.ds(i * packed, packed)
-            total[rows, :] += dot1(act[pl.ds(0, packed), pl.ds(i * hc, hc)], w)
-        total[...] += dot1(act[pl.ds(packed, half), :], wc[pl.ds(pl.multiple_of(b * cc, cc), cc), :])
-
-    for way in range(2):
-        @pl.when(sends(0, way))
-        def _():
-            along(0, way).start()
+    for i in range(1, pieces):
+        begin(i)
     for j in range(m - 1):
-        across(0, j, s).start()
+        across(0, j, s, 1).start()
     total[...] = jnp.zeros_like(total)
+    pass_on(0, 0)
     add(s, own.at[t], wm_ref, wc_ref)
     for copy in outs[everyone - 1 :]:
         copy.wait()
 
     def from_mates(index, b):
         for j in range(m - 1):
-            across(index, j, b).wait_recv()
+            for i in range(2):
+                across(index, j, b, i).wait_recv()
             add(b, mates_act.at[j, b], wm_in.at[j], wc_in.at[j])
-            across(index, j, b).wait_send()
+            for i in range(2):
+                across(index, j, b, i).wait_send()
 
     for k in range(n - 1):
+        if k > 0:
+            pass_on(k, 0)
+        for i in range(1, pieces):
+            pass_on(k, i)
         for way in range(2):
             @pl.when(gets(k, way))
             def _():
                 b = s - 1 - k if way == 0 else s + 1 + k
-                remote(around.at[b], around.at[b], asend.at[way, k], arecv.at[way, k], {"sp": b}).wait_recv()
-                if k + 1 < n - 1:
-                    @pl.when(sends(k + 1, way))
-                    def _():
-                        along(k + 1, way).start()
-                for j in range(m - 1):
-                    across(1 + 2 * k + way, j, b).start()
                 add(b, around.at[b, t], wm_ref, wc_ref)
         if k == 0:
             from_mates(0, s)
@@ -477,7 +558,8 @@
         for way in range(2):
             @pl.when(sends(k, way))
             def _():
-                along(k, way).wait_send()
+                for i in range(pieces):
+                    along(k, way, i).wait_send()
     block[...] = total[...].astype(bf16)
     mine = out_ref.at[:, pl.ds(pl.multiple_of(s * columns, columns), columns)]
     keep = pltpu.make_async_copy(block.at[pl.ds(s * share, share)], mine, local.at[0])
@@ -521,8 +603,8 @@
             dma((1,)),
             dma((n * m - 1,)), dma((n * m - 1,)),
             dma((2, mates)), dma((2, mates)),
-            dma((2, hops)), dma((2, hops)),
-            dma((2 * n - 1, mates)), dma((2 * n - 1, mates)),
+            dma((2, hops, m + 1)), dma((2, hops, m + 1)),
+            dma((2 * n - 1, mates, 2)), dma((2 * n - 1, mates, 2)),
             dma((hops,)), dma((hops,)),
         ],
         compiler_params=pltpu.CompilerParams(collective_id=1, has_side_effects=True),
@@ -776,8 +858,9 @@
     pointwise_value_weight, pointwise_gate_weight, depthwise_taps_weight, channel_norm_scale,
     mixer_output_weight, convolution_output_weight,
 ):
-    n, m = lax.axis_size("sp"), lax.axis_size("tp")
-    if query_matrix.shape[1] % (n * GROUP) or pointwise_value_weight.shape[1] % (n * 128):
+    n, m, nf = lax.axis_size("sp"), lax.axis_size("tp"), lax.axis_size("fs")
+    lanes = query_matrix.shape[1] % (n * GROUP) or pointwise_value_weight.shape[1] % (n * 128)
+    if lanes or query_matrix.shape[0] % (nf * 16):
         return spread_device(
             inputs, input_norm_scale, query_matrix, key_matrix, value_matrix,
             decay_down_weight, decay_up_weight, decay_bias_base, decay_position_offset, extra_log_decay,
@@ -787,12 +870,10 @@
         )
     x = inputs[0]
     rows = x.shape[0]
-    depth = query_matrix.shape[0]
     hc, cc = query_matrix.shape[1] // n, pointwise_value_weight.shape[1] // n
     parts = [query_matrix, key_matrix, pointwise_value_weight, pointwise_gate_weight, value_matrix]
-    w = jnp.concatenate([part.reshape(depth, n, -1) for part in parts], axis=2).transpose(1, 0, 2)
     e = jnp.concatenate([decay_position_offset[0], extra_log_decay[0]], axis=1).T
-    everything, columns, shifts = collect(n, m, x, w, e)
+    everything, columns, shifts = collect(n, m, nf, x, parts, e)
     mixed, conv, sums = mix(
         n, m, hc, cc, rows,
         everything, input_norm_scale[None], columns, shifts,

time: 153 us -> 104 us (0.68)
  Pallas kernels: 141 us -> 101 us
  local copies, waits for them, and re-layouts: 9.9 us -> 1.67 us
    pallas_call x1, Pallas kernels: 73.8 us -> 39.6 us  [collect(): pl.pallas_call(functools.partial(collect_kernel, n, m, nf, cut), out_shap...]
    pallas_call x1, Pallas kernels: 35.5 us -> 29.1 us  [output(): pl.pallas_call(functools.partial(output_kernel, n, m, hc, cc, pack), out_...]
    concatenate x1 -> x0, local copies, waits for them, and re-layouts: 4.11 us -> none  [per_device(): jnp.concatenate([part.reshape(depth, n, -1) for part in parts], axis=2)]
    unnamed x12 -> x1, local copies, waits for them, and re-layouts: 4.43 us -> 1.67 us
where the time goes in v1:
time: 104 us
  Pallas kernels  101 us (97%)
  local copies, waits for them, and re-layouts  1.67 us (2%)
  other arithmetic  1.3 us (1%)
    pallas_call x1, Pallas kernels, collect(): pl.pallas_call(functools.partial(collect_kernel, n, m, nf, cut), out_shap...  39.6 us
    pallas_call x1, Pallas kernels, mix(): pl.pallas_call(functools.partial(mix_kernel, n, m, hc, cc, rows), out_sha...  32.2 us
    pallas_call x1, Pallas kernels, output(): pl.pallas_call(functools.partial(output_kernel, n, m, hc, cc, pack), out_...  29.1 us

profile of v1, /device:TPU:0, one launch (start us, length us, event | category | flops | bytes accessed | tf_op | source)
XLA Modules:
  0.0 103.9 jit_solution(3320111539206997176)
XLA Ops:
  0.0 1.3 %maximum_bitcast_fusion.e_ref = f32[8,128]{1,0:T(8,128)} fusion(f32[128,4]{0,1:T(4,128)} %bitcast.15, f32[128,4]{0,1:T(4,128)} %bitcast.16), kind=kLoop, calls=%fused_computation | loop fusion | flops 1024 | bytes 8192 | tf_op jit(solution)/shard_map/transpose | solution.py:875
  1.3 39.6 %shard_map.199 = (bf16[512,2048]{1,0:T(8,128)(2,1)}, bf16[2048,448]{1,0:T(8,128)(2,1)}, f32[4,8,128]{2,1,0:T(8,128)}) custom-call(bf16[128,1024]{1,0:T(8,128)(2,1)} %bitcast.12, bf16[512,256]{1,0:T(8,128)(2,1)} %q_ref.1, bf16[512,256]{1,0:T(8,128)(2,1)} %k_ref.1, bf16[512,512]{1,0:T(8,128)(2,1)} %pv_ref.1, bf16[512,512]{1,0:T(8,128)(2,1)} %pg_ref.1, ...), custom_call_target="tpu_custom_call" | custom-call | tf_op jit(solution)/shard_map/pallas_call | solution.py:195
  40.9 32.2 %shard_map.200 = (bf16[2,256,64]{2,1,0:T(8,128)(2,1)}, f32[512,128]{1,0:T(8,128)}, f32[8,512]{1,0:T(8,128)}) custom-call(bf16[512,2048]{1,0:T(8,128)(2,1)} %get-tuple-element.11.x_ref, f32[1,2048]{1,0:T(1,128)} %bitcast.13, bf16[2048,448]{1,0:T(8,128)(2,1)} %get-tuple-element.12.w_ref, f32[4,8,128]{2,1,0:T(8,128)} %get-tuple-element.13.e_ref, ...), custom_call_target="tpu_custom_call" | custom-call | tf_op jit(solution)/shard_map/pallas_call | solution.py:384
  73.2 29.1 %shard_map.201 = bf16[64,2048]{1,0:T(8,128)(2,1)} custom-call(bf16[2,256,64]{2,1,0:T(8,128)(2,1)} %get-tuple-element.14.mix_ref, f32[512,128]{1,0:T(8,128)} %get-tuple-element.15.conv_ref, f32[8,512]{1,0:T(8,128)} %get-tuple-element.16.sums_ref, f32[1,512]{1,0:T(1,128)} %bitcast.14, bf16[256,512]{1,0:T(8,128)(2,1)} %wm_ref.1, bf16[512,512]{1,0:T(8,128)(2,1)} %wc_ref.1), custom_call_target="tpu_custom_call" | custom-call | tf_op jit(solution)/shard_map/pallas_call | solution.py:589
  102.3 1.7 %copy.23 = bf16[1,64,2048]{2,1,0:T(8,128)(2,1)} copy(bf16[1,64,2048]{2,1,0:T(8,128)(2,1)} %bitcast.11) | data formatting | bytes 524288

commit v2 on v1

--- a/solution.py
+++ b/solution.py
@@ -286,8 +286,9 @@
         pick_offset = (erow == s * heads + h).astype(f32)
         pick_extra = (erow == local_heads + s * heads + h).astype(f32)
 
-        @pl.loop(0, length // size)
-        def _(i):
+        together = 2 if (length // size) % 2 == 0 else 1
+
+        def prepare(i):
             at = pl.ds(pl.multiple_of(i * size, size), size)
             inner = rows // size
             if inner == 1:
@@ -305,46 +306,59 @@
             unit = k * lax.rsqrt(jnp.sum(k * k, axis=-1, keepdims=True) + 1e-06)
             rated = unit * rate
             total = exact_left(whole, lw)
+            middle = 0.5 * total
+            work = []
             for d in range(2):
                 strict = same & ((ti > tj) if d == 0 else (ti < tj))
                 upto = same & ((ti >= tj) if d == 0 else (ti <= tj))
                 g = exact_left(upto.astype(f32).astype(bf16), lw)
                 before = g - lw
-                middle = 0.5 * total
                 ahead = jnp.exp(middle - g)
-                left = halves(jnp.concatenate([unit * jnp.exp(before - middle), q * jnp.exp(g - middle)], axis=0))
                 right = halves(jnp.concatenate([rated * ahead, k * ahead], axis=0))
-                scores = dot3(left, right, NT)
-                a_ur = jnp.where(strict, scores[:size, :size], 0.0)
-                a_uk = jnp.where(strict, scores[:size, size:], 0.0)
-                a_qr = jnp.where(upto, scores[size:, :size], 0.0)
-                a_qk = jnp.where(upto, scores[size:, size:], 0.0)
-                width = 1
+                near = dot3(unit * jnp.exp(before - middle), right, NT)
+                seen = dot1((q * jnp.exp(g - middle)).astype(bf16), right[0], NT)
+                a_ur = jnp.where(strict, near[:, :size], 0.0)
+                a_uk = jnp.where(strict, near[:, size:], 0.0)
+                a_qr = jnp.where(upto, seen[:, :size], 0.0).astype(bf16)
+                a_qk = jnp.where(upto, seen[:, size:], 0.0).astype(bf16)
                 inverse = eye - jnp.where((ti // 2 == tj // 2), a_ur, 0.0)
-                width = 2
-                while width < CHUNK:
-                    part = jnp.where(
-                        (ti // (2 * width) == tj // (2 * width)) & (ti // width != tj // width), a_ur, 0.0
-                    )
-                    pair = halves(inverse)
-                    inverse = inverse - dot3(dot3(pair, part), pair)
-                    width *= 2
-                a_kv = halves(jnp.concatenate([a_uk, a_qk], axis=0))
-                both = dot1(a_kv[0], vb) + dot1(a_kv[1], vb)
-                wy = dot3(inverse, jnp.concatenate([unit * jnp.exp(before), both[:size]], axis=1))
-                far = dot3(a_qr, wy)
-                qe[d, at, :] = q * jnp.exp(g) - far[:, :GROUP]
-                oi[d, at, :] = both[size:] - far[:, GROUP:]
-                tail = jnp.exp(total - g)
-                r_end, k_end = rated * tail, k * tail
-                for c in range(per):
-                    cut = slice(c * CHUNK, (c + 1) * CHUNK)
-                    moved = dot3(wy[cut], r_end[cut], TN)
-                    ke = halves(k_end[cut])
-                    came = dot1(vb[cut], ke[0], TN) + dot1(vb[cut], ke[1], TN)
-                    decay = jnp.exp(total[c * CHUNK : c * CHUNK + 1])
-                    maps[d, i * per + c] = small_eye * decay - moved[:GROUP]
-                    adds[d, i * per + c] = came - moved[GROUP:]
+                work.append((i, d, at, a_ur, a_uk, a_qr, a_qk, inverse, g, before, total, q, k, vb, unit, rated))
+            return work
+
+        def finish(item, inverse):
+            i, d, at, a_ur, a_uk, a_qr, a_qk, _, g, before, total, q, k, vb, unit, rated = item
+            a_uk = halves(a_uk)
+            pulled = dot1(a_uk[0], vb) + dot1(a_uk[1], vb)
+            wy = dot3(inverse, jnp.concatenate([unit * jnp.exp(before), pulled], axis=1))
+            far = dot1(a_qr, wy.astype(bf16))
+            qe[d, at, :] = q * jnp.exp(g) - far[:, :GROUP]
+            oi[d, at, :] = dot1(a_qk, vb) - far[:, GROUP:]
+            tail = jnp.exp(total - g)
+            r_end, k_end = rated * tail, k * tail
+            for c in range(per):
+                cut = slice(c * CHUNK, (c + 1) * CHUNK)
+                moved = dot3(wy[cut], r_end[cut], TN)
+                ke = halves(k_end[cut])
+                came = dot1(vb[cut], ke[0], TN) + dot1(vb[cut], ke[1], TN)
+                decay = jnp.exp(total[c * CHUNK : c * CHUNK + 1])
+                maps[d, i * per + c] = small_eye * decay - moved[:GROUP]
+                adds[d, i * per + c] = came - moved[GROUP:]
+
+        @pl.loop(0, length // size // together)
+        def _(step_at):
+            work = []
+            for u in range(together):
+                work += prepare(step_at * together + u)
+            inverses = [item[7] for item in work]
+            width = 2
+            while width < CHUNK:
+                level = (ti // (2 * width) == tj // (2 * width)) & (ti // width != tj // width)
+                pairs = [halves(x) for x in inverses]
+                firsts = [dot3(p, jnp.where(level, item[3], 0.0)) for p, item in zip(pairs, work)]
+                inverses = [x - dot3(y, p) for x, y, p in zip(inverses, firsts, pairs)]
+                width *= 2
+            for item, inverse in zip(work, inverses):
+                finish(item, inverse)
 
         chunks = length // CHUNK
         now = [st_ref[0, 0, s * heads + h], st_ref[0, 1, s * heads + h]]

time: 104 us -> 93.9 us (0.903)
  Pallas kernels: 101 us -> 90.7 us
    pallas_call x1, Pallas kernels: 32.2 us -> 22 us  [mix(): pl.pallas_call(functools.partial(mix_kernel, n, m, hc, cc, rows), out_sha...]
where the time goes in v2:
time: 93.9 us; the launch traced here: 93.7 us
  Pallas kernels  90.7 us (97%)
  local copies, waits for them, and re-layouts  1.67 us (2%)
  other arithmetic  1.3 us (1%)
    pallas_call x1, Pallas kernels, collect(): pl.pallas_call(functools.partial(collect_kernel, n, m, nf, cut), out_shap...  39.6 us
    pallas_call x1, Pallas kernels, output(): pl.pallas_call(functools.partial(output_kernel, n, m, hc, cc, pack), out_...  29.1 us
    pallas_call x1, Pallas kernels, mix(): pl.pallas_call(functools.partial(mix_kernel, n, m, hc, cc, rows), out_sha...  22 us

profile of v2, /device:TPU:0, one launch (start us, length us, event | category | flops | bytes accessed | tf_op | source)
XLA Modules:
  0.0 93.7 jit_solution(1690668934236601976)
XLA Ops:
  0.0 1.3 %maximum_bitcast_fusion.e_ref = f32[8,128]{1,0:T(8,128)} fusion(f32[128,4]{0,1:T(4,128)} %bitcast.15, f32[128,4]{0,1:T(4,128)} %bitcast.16), kind=kLoop, calls=%fused_computation | loop fusion | flops 1024 | bytes 8192 | tf_op jit(solution)/shard_map/transpose | solution.py:889
  1.3 39.6 %shard_map.199 = (bf16[512,2048]{1,0:T(8,128)(2,1)}, bf16[2048,448]{1,0:T(8,128)(2,1)}, f32[4,8,128]{2,1,0:T(8,128)}) custom-call(bf16[128,1024]{1,0:T(8,128)(2,1)} %bitcast.12, bf16[512,256]{1,0:T(8,128)(2,1)} %q_ref.1, bf16[512,256]{1,0:T(8,128)(2,1)} %k_ref.1, bf16[512,512]{1,0:T(8,128)(2,1)} %pv_ref.1, bf16[512,512]{1,0:T(8,128)(2,1)} %pg_ref.1, ...), custom_call_target="tpu_custom_call" | custom-call | tf_op jit(solution)/shard_map/pallas_call | solution.py:195
  40.9 22.0 %shard_map.200 = (bf16[2,256,64]{2,1,0:T(8,128)(2,1)}, f32[512,128]{1,0:T(8,128)}, f32[8,512]{1,0:T(8,128)}) custom-call(bf16[512,2048]{1,0:T(8,128)(2,1)} %get-tuple-element.11.x_ref, f32[1,2048]{1,0:T(1,128)} %bitcast.13, bf16[2048,448]{1,0:T(8,128)(2,1)} %get-tuple-element.12.w_ref, f32[4,8,128]{2,1,0:T(8,128)} %get-tuple-element.13.e_ref, ...), custom_call_target="tpu_custom_call" | custom-call | tf_op jit(solution)/shard_map/pallas_call | solution.py:398
  63.0 29.1 %shard_map.201 = bf16[64,2048]{1,0:T(8,128)(2,1)} custom-call(bf16[2,256,64]{2,1,0:T(8,128)(2,1)} %get-tuple-element.14.mix_ref, f32[512,128]{1,0:T(8,128)} %get-tuple-element.15.conv_ref, f32[8,512]{1,0:T(8,128)} %get-tuple-element.16.sums_ref, f32[1,512]{1,0:T(1,128)} %bitcast.14, bf16[256,512]{1,0:T(8,128)(2,1)} %wm_ref.1, bf16[512,512]{1,0:T(8,128)(2,1)} %wc_ref.1), custom_call_target="tpu_custom_call" | custom-call | tf_op jit(solution)/shard_map/pallas_call | solution.py:603
  92.0 1.7 %copy.23 = bf16[1,64,2048]{2,1,0:T(8,128)(2,1)} copy(bf16[1,64,2048]{2,1,0:T(8,128)(2,1)} %bitcast.11) | data formatting | bytes 524288
